TPU v7x, 512 devices: a whole 4x4x16 slice. The times are simulated.
512 devices in a mesh: sp: 128 (over z, x, core), tp: 4 (over y).
Axes of the slice: x: 4, y: 4, z: 16, core: 2. Of those that a mesh axis runs over, the one named last changes fastest.
Arguments:
- tokens: bfloat16 [32768, 2048], P('sp'), may hold values from -6 to 6
- documents: int32 [32768], P('sp'), may hold values from 0 to 63, never falling along the last dimension, each value on 1 to 1024 neighbouring positions
- norm_gain: float32 [1, 2048], replicated, may hold values from 0.1 to 1.9
- w_query: bfloat16 [1, 2048, 2048], P(None, 'sp', 'tp'), may hold values from -0.125 to 0.125
- w_key: bfloat16 [1, 2048, 2048], P(None, 'sp', 'tp'), may hold values from -0.125 to 0.125
- w_value: bfloat16 [1, 2048, 2048], P(None, 'sp', 'tp'), may hold values from -0.125 to 0.125
- w_out: bfloat16 [1, 2048, 2048], P(None, None, 'sp'), may hold values from -0.59765625 to 0.59765625
- rel_bias: float32 [1, 32, 257], P(None, 'tp'), may hold values from -8 to 240
Outputs:
- mixed: bfloat16 [32768, 2048], P('sp')
Inputs may be any that keep to these rules, and one draw needn't show every extreme that they name: `documents`: document numbers never fall along the sequence; a document has 1 to 1024 positions.
All inputs are finite; a program needn't handle non-finite values.
Results may differ from a plain program's by a relative error of at most 0.007.
Values may be sent and summed in bfloat16 or wider, within the bound.
No kernel may reach another device: no remote copies, remote signals or barrier semaphores. Data moves between devices by JAX's collectives and lax.ppermute only.
A program may use at most 128 MiB of HBM per device.

v0:
```python
import jax
import jax.numpy as jnp
from jax import lax
from jax.sharding import Mesh
from jax.sharding import PartitionSpec as P

HEAD_DIM = 64
SEG = 64
LEFT = 4
REL_CLIP = 128
SP = ("sp_0", "sp_1", "sp_2")
EPS = 1e-06


def passed_along(x, axis, by):
    length = lax.axis_size(axis)
    pairs = [(i, i + by) for i in range(length) if 0 <= i + by < length]
    return lax.ppermute(x, axis, pairs)


def in_one_piece(arrays, axis, dim, along):
    ends, at = ([], 0)
    for a in arrays[:-1]:
        at += a.shape[along]
        ends.append(at)
    both = jnp.concatenate(arrays, axis=along)
    return tuple(jnp.split(lax.all_gather(both, axis, axis=dim, tiled=True), ends, axis=along))


def laid_out(pieces, dim):
    shape = list(pieces.shape[1:])
    shape[dim] *= pieces.shape[0]
    return jnp.moveaxis(pieces, 0, dim).reshape(shape)


def from_everyone(x, axis):
    length = lax.axis_size(axis)
    return lax.all_to_all(jnp.broadcast_to(x[None], (length, *x.shape)), axis, 0, 0, tiled=True)


def collect(x, axis, dim):
    return laid_out(from_everyone(x, axis), dim)


def gather_in_order(x, axes, order):
    pieces = x[None]
    for k in order:
        pieces = lax.all_gather(pieces, axes[k], axis=0, tiled=True)
    held = [lax.axis_size(axes[k]) for k in reversed(order)]
    pieces = pieces.reshape(*held, *x.shape)
    turned = sorted(range(len(order)), key=lambda place: order[len(order) - 1 - place])
    return pieces.transpose(*turned, *range(len(order), pieces.ndim)).reshape(-1, *x.shape)


def gather_axes(x, axes, order, dim):
    return laid_out(gather_in_order(x, axes, order), dim)


def banded_bias(bias_table, query_rows, key_rows, reach_rows):
    span_len = query_rows + key_rows - 1
    steps_back = jnp.arange(span_len, dtype=jnp.int32) - (key_rows - 1) + reach_rows
    lookup = jnp.clip(steps_back, -REL_CLIP, REL_CLIP) + REL_CLIP
    bias_line = jnp.take(bias_table, lookup, axis=1)
    reversed_line = bias_line[:, ::-1]
    repeated = jnp.tile(reversed_line, (1, query_rows))
    skewed = repeated[:, query_rows - 1 : query_rows - 1 + query_rows * (span_len - 1)]
    skewed = skewed.reshape(bias_table.shape[0], query_rows, span_len - 1)
    return skewed[:, :, :key_rows]


def attend(queries, keys_all, values_all, query_pos, key_pos, query_doc, key_doc, bias_table):
    query_rows = queries.shape[0]
    key_rows = keys_all.shape[0]
    reach_rows = key_rows - query_rows
    scores = jnp.einsum(
        "qhe,khe->hqk", queries, keys_all, preferred_element_type=jnp.float32
    ) * HEAD_DIM ** (-0.5)
    scores = scores + banded_bias(bias_table, query_rows, key_rows, reach_rows)
    query_seg = query_pos // SEG
    key_seg = key_pos // SEG
    allowed = (
        (key_pos[None, :] >= 0)
        & (key_seg[None, :] <= query_seg[:, None])
        & (key_seg[None, :] >= query_seg[:, None] - LEFT)
        & (key_doc[None, :] == query_doc[:, None])
    )
    scores = jnp.where(allowed[None], scores, -1e30)
    peak = jnp.max(scores, axis=-1, keepdims=True)
    raised = jnp.exp(scores - peak)
    weights_bf = (raised / jnp.sum(raised, axis=-1, keepdims=True)).astype(jnp.bfloat16)
    return jnp.einsum(
        "hqk,khe->qhe", weights_bf, values_all, preferred_element_type=jnp.float32
    ).astype(jnp.bfloat16)


def body(tokens, documents, norm_gain, w_query, w_key, w_value, w_out, rel_bias):
    local_rows = tokens.shape[0]
    reach_rows = LEFT * SEG
    width_local = w_query.shape[2]
    heads_local = width_local // HEAD_DIM
    offset = lax.axis_index(SP) * local_rows
    query_pos = offset + jnp.arange(local_rows, dtype=jnp.int32)
    key_pos = offset - reach_rows + jnp.arange(reach_rows + local_rows, dtype=jnp.int32)
    widened = tokens.astype(jnp.float32)
    normed = (
        widened
        * lax.rsqrt(jnp.mean(widened * widened, axis=-1, keepdims=True) + EPS)
        * norm_gain[0]
    ).astype(jnp.bfloat16)
    before, prior_docs = passed_along((normed, documents), SP, 1)
    extended = jnp.concatenate([before, normed], axis=0)
    pieces = in_one_piece((w_query[0], w_key[0], w_value[0]), SP, 0, 1)
    query_sum = jnp.dot(normed, pieces[0], preferred_element_type=jnp.float32)
    key_sum = jnp.dot(extended, pieces[1], preferred_element_type=jnp.float32)
    value_sum = jnp.dot(extended, pieces[2], preferred_element_type=jnp.float32)
    queries = query_sum.astype(jnp.bfloat16)
    keys_all = key_sum.astype(jnp.bfloat16)
    values_all = value_sum.astype(jnp.bfloat16)
    key_doc = jnp.concatenate([prior_docs, documents], axis=0)
    attended = attend(
        queries.reshape(local_rows, heads_local, HEAD_DIM),
        keys_all.reshape(reach_rows + local_rows, heads_local, HEAD_DIM),
        values_all.reshape(reach_rows + local_rows, heads_local, HEAD_DIM),
        query_pos,
        key_pos,
        documents,
        key_doc,
        rel_bias[0],
    ).reshape(local_rows, width_local)
    all_heads = collect(attended, "tp", 1)
    return (
        widened
        + jnp.dot(
            all_heads, gather_axes(w_out[0], SP, (1, 0, 2), 1), preferred_element_type=jnp.float32
        )
    ).astype(jnp.bfloat16)


def solution(mesh):
    split = Mesh(mesh.devices.reshape(16, 4, 2, mesh.shape["tp"]), ("sp_0", "sp_1", "sp_2", "tp"))
    placed = (
        P(SP, None),
        P(SP),
        P(),
        P(None, SP, "tp"),
        P(None, SP, "tp"),
        P(None, SP, "tp"),
        P(None, None, SP),
        P(None, "tp", None),
    )
    return jax.shard_map(body, mesh=split, in_specs=placed, out_specs=P(SP, None), check_vma=False)
```

profile of v0, /device:TPU:32, one launch (start us, length us, event | category | flops | bytes accessed | tf_op | source)
XLA Modules:
  0.0 303.6 jit_solution(17535925062422447760)
XLA Ops:
  6.5 0.0 copy-start.1
  6.5 0.0 copy-start.3
  6.5 0.0 copy-start.4
  6.5 0.0 copy-start.2
  6.5 0.0 all-gather.6.cloned.1.call-start
  6.6 14.3 %all_gather.13 = bf16[4,2048,16]{1,2,0:T(8,128)(2,1)} all-gather(bf16[1,2048,16]{1,2,0:T(8,128)(2,1)} %param.14), channel_id=1, replica_groups=mesh['sp_0'=16,'sp_1'=4,'sp_2'=2,'tp'=4] {'sp_1'}, dimensions={0}, use_global_device_ids=true | all-gather | bytes 327680 | tf_op jit(solution)/shard_map/all_gather | solution.py:48
  20.9 0.0 all-gather.6.cloned.1.call-update
  21.0 0.0 all-gather.4.cloned.1.call-start
  21.0 1.4 pad_maximum_fusion.7
  22.4 0.0 all-gather.4.cloned.1.call-update
  22.4 0.0 all-gather.8.cloned.1.call-start
  22.4 79.5 %all-gather.6.cloned.1.call-done = bf16[64,2048,16]{1,2,0:T(8,128)(2,1)} async-done(((bf16[4,2048,16]{1,2,0:T(8,128)(2,1)}), bf16[64,2048,16]{1,2,0:T(8,128)(2,1)}) %all-gather.6.cloned.1.call-update) | async-done | bytes 4194320 | tf_op jit(solution)/shard_map/all_gather | solution.py:48
  101.9 0.0 all-gather.8.cloned.1.call-update
  101.9 0.0 copy-done.1
  102.0 0.3 fusion.3
  102.2 0.0 copy-done.3
  102.3 1.3 fusion.5
  103.5 1.9 collective-permute-start
  105.5 0.0 copy-done.4
  105.5 3.5 %collective-permute-start.1 = (s32[256]{0:T(256)S(1)}, s32[256]{0:T(256)S(1)}, u32[]{:S(2)}, u32[]{:S(2)}) collective-permute-start(s32[256]{0:T(256)S(1)} %copy-done.4), channel_id=1, source_target_pairs={{0,4},{4,8},{8,12},{12,16},{16,20},{20,24},{24,28},{28,32},{32,36}... | collective-permute-start | bytes 3080 | tf_op jit(solution)/shard_map/ppermute | solution.py:18
  109.1 0.0 copy-done.2
  109.1 0.1 copy.21
  109.2 1.6 gather_fusion
  110.8 0.2 select_bitcast_fusion
  111.0 0.5 rev.3
  111.4 0.1 copy.22
  111.6 3.2 %tile.4 = f32[8,256,767]{2,1,0:T(8,128)} broadcast(f32[8,767]{1,0:T(8,128)S(1)} %copy.22), dimensions={0,2} | broadcast | bytes 6307808 | tf_op jit(solution)/shard_map/tile | solution.py:65
  114.7 8.8 %tile.10 = f32[8,196352]{1,0:T(8,128)} reshape(f32[8,256,767]{2,1,0:T(8,128)} %tile.4) | data formatting | bytes 12566528 | tf_op jit(solution)/shard_map/tile | solution.py:65
  123.5 5.5 %slice.10 = f32[8,196096]{1,0:T(8,128)} slice(f32[8,196352]{1,0:T(8,128)} %tile.10), slice={[0:8], [255:196351]} | slice | bytes 12550144 | tf_op jit(solution)/shard_map/slice | solution.py:66
  128.9 12.4 %reshape.213 = f32[8,256,766]{2,1,0:T(8,128)} reshape(f32[8,196096]{1,0:T(8,128)} %slice.10) | data formatting | bytes 12550144 | tf_op jit(solution)/shard_map/reshape | solution.py:67
  141.3 0.0 collective-permute-done.1
  141.3 0.3 compare_and_fusion
  141.6 104.4 %all-gather.4.cloned.1.call-done = bf16[2048,1536]{1,0:T(8,128)(2,1)} async-done(((bf16[16,1536]{1,0:T(8,128)(2,1)}), bf16[2048,1536]{1,0:T(8,128)(2,1)}) %all-gather.4.cloned.1.call-update) | async-done | bytes 6291472 | tf_op jit(solution)/shard_map/all_gather | solution.py:27
  246.0 0.0 slice-start
  246.0 3.5 %fusion.20 = bf16[256,512]{1,0:T(8,128)(2,1)} fusion(bf16[256,2048]{1,0:T(8,128)(2,1)} %fusion.5, bf16[2048,1536]{1,0:T(8,128)(2,1)} %all-gather.4.cloned.1.call-done), kind=kOutput, calls=%fused_computation.24 | convolution fusion | flops 537001984 | bytes 3407872 | tf_op jit(solution)/shard_map/dot_general | solution.py:113
  249.5 1.1 copy.20
  250.6 0.0 slice-start.1
  250.6 0.0 collective-permute-done
  250.6 3.7 %fusion.16 = bf16[512,512]{0,1:T(8,128)(2,1)S(1)} fusion(bf16[2048,1536]{1,0:T(8,128)(2,1)} %all-gather.4.cloned.1.call-done, bf16[256,2048]{1,0:T(8,128)(2,1)} %fusion.5, bf16[256,2048]{1,0:T(8,128)(2,1)} %collective-permute-done), kind=kOutput, calls=%fused_computation.22 | convolution fusion | flops 1078198272 | bytes 4718592 | tf_op jit(solution)/shard_map/dot_general | solution.py:114
  254.3 0.0 slice-done
  254.3 0.0 slice-done.1
  254.3 0.9 fusion.1
  255.2 0.0 copy-start
  255.2 1.7 fusion.34
  257.0 3.6 %fusion.13 = bf16[512,512]{0,1:T(8,128)(2,1)S(1)} fusion(bf16[2048,1536]{1,0:T(8,128)(2,1)} %all-gather.4.cloned.1.call-done, bf16[256,2048]{1,0:T(8,128)(2,1)} %fusion.5, bf16[256,2048]{1,0:T(8,128)(2,1)} %collective-permute-done), kind=kOutput, calls=%fused_computation.21 | convolution fusion | flops 1078198272 | bytes 4718592 | tf_op jit(solution)/shard_map/dot_general | solution.py:115
  260.6 0.0 copy-done
  260.6 8.9 %fusion.19 = bf16[8,64,256]{2,1,0:T(8,128)(2,1)S(1)} fusion(bf16[512,8,64]{0,2,1:T(8,128)(2,1)S(1)} %bitcast.45, f32[8,256]{1,0:T(8,128)S(1)} %fusion.34, f32[8,256,512]{2,1,0:T(8,128)} %copy-done), kind=kOutput, calls=%fused_computation.23 | convolution fusion | flops 137497088 | bytes 4988928 | tf_op jit(solution)/shard_map/hqk,khe->qhe/dot_general | solution.py:91
  269.5 1.0 broadcast_in_dim.45
  270.5 4.3 %all-to-all-start = ((bf16[4,256,512]{1,2,0:T(8,128)(2,1)}), bf16[4,256,512]{1,2,0:T(8,128)(2,1)S(1)}, u32[]{:S(2)}, u32[]{:S(2)}) async-start(bf16[4,256,512]{1,2,0:T(8,128)(2,1)} %broadcast_in_dim.45), calls=%async_computation | async-start | bytes 2097152 | tf_op jit(solution)/shard_map/all_to_all | solution.py:38
  274.8 0.0 all-gather.8.cloned.1.call-done
  274.8 8.2 %copy.23 = bf16[16,4,2,2048,16]{3,4,2,1,0:T(8,128)(2,1)} copy(bf16[16,4,2,2048,16]{3,4,1,0,2:T(8,128)(2,1)} %bitcast.34) | data formatting | bytes 16777216 | tf_op jit(solution)/shard_map/transpose | solution.py:52
  283.1 7.3 %all-to-all-done = bf16[4,256,512]{1,2,0:T(8,128)(2,1)S(1)} async-done(((bf16[4,256,512]{1,2,0:T(8,128)(2,1)}), bf16[4,256,512]{1,2,0:T(8,128)(2,1)S(1)}, u32[]{:S(2)}, u32[]{:S(2)}) %all-to-all-start) | async-done | bytes 1048608 | tf_op jit(solution)/shard_map/all_to_all | solution.py:38
  290.4 6.7 %fusion.2 = bf16[256,2048]{1,0:T(8,128)(2,1)} fusion(bf16[256,2048]{0,1:T(8,128)(2,1)S(1)} %bitcast.37, bf16[2048,2048]{0,1:T(8,128)(2,1)} %bitcast.35, bf16[256,2048]{1,0:T(8,128)(2,1)S(1)} %copy-done.1), kind=kOutput, calls=%fused_computation.9 | convolution fusion | flops 2149056512 | bytes 11534336 | tf_op jit(solution)/shard_map/dot_general | solution.py:133
  (9 shorter events, 0.1 us)
Async XLA Ops:
  6.5 95.4 %copy-start.1 = (bf16[256,2048]{1,0:T(8,128)(2,1)S(1)}, bf16[256,2048]{1,0:T(8,128)(2,1)}, u32[]{:S(2)}) copy-start(bf16[256,2048]{1,0:T(8,128)(2,1)} %param.8) | copy-start | bytes 3145732
  6.5 95.7 %copy-start.3 = (f32[1,2048]{1,0:T(1,128)S(1)}, f32[1,2048]{1,0:T(1,128)}, u32[]{:S(2)}) copy-start(f32[1,2048]{1,0:T(1,128)} %param.10) | copy-start | bytes 24580
  6.5 98.9 %copy-start.4 = (s32[256]{0:T(256)S(1)}, s32[256]{0:T(256)}, u32[]{:S(2)}) copy-start(s32[256]{0:T(256)} %param.9) | copy-start | bytes 3076
  6.5 102.5 %copy-start.2 = (f32[1,8,257]{2,1,0:T(8,128)S(1)}, f32[1,8,257]{2,1,0:T(8,128)}, u32[]{:S(2)}) copy-start(f32[1,8,257]{2,1,0:T(8,128)} %param.15) | copy-start | bytes 24676
  6.5 95.4 %all-gather.6.cloned.1.call-start = ((), (), s32[]{:S(2)}) async-start(), calls=%async_computation.2 | async-start | bytes 4456448 | tf_op jit(solution)/shard_map/all_gather | solution.py:48
  21.0 225.1 %all-gather.4.cloned.1.call-start = ((), (), s32[]{:S(2)}) async-start(), calls=%async_computation.1 | async-start | bytes 6340608 | tf_op jit(solution)/shard_map/all_gather | solution.py:27
  22.4 252.4 %all-gather.8.cloned.1.call-start = ((), (), s32[]{:S(2)}) async-start(), calls=%async_computation.3 | async-start | bytes 12582912 | tf_op jit(solution)/shard_map/all_gather | solution.py:48
  103.5 147.0 %collective-permute-start = (bf16[256,2048]{1,0:T(8,128)(2,1)}, bf16[256,2048]{1,0:T(8,128)(2,1)}, u32[]{:S(2)}, u32[]{:S(2)}) collective-permute-start(bf16[256,2048]{1,0:T(8,128)(2,1)} %fusion.5), channel_id=1, source_target_pairs={{0,4},{4,8},{8,12},{12,16},{16,20},{20,24},{24,28},{28,32},{32,36}... | collective-permute-start | bytes 3145736 | tf_op jit(solution)/shard_map/ppermute | solution.py:18
  105.5 35.9 %collective-permute-start.1 = (s32[256]{0:T(256)S(1)}, s32[256]{0:T(256)S(1)}, u32[]{:S(2)}, u32[]{:S(2)}) collective-permute-start(s32[256]{0:T(256)S(1)} %copy-done.4), channel_id=1, source_target_pairs={{0,4},{4,8},{8,12},{12,16},{16,20},{20,24},{24,28},{28,32},{32,36}... | collective-permute-start | bytes 3080 | tf_op jit(solution)/shard_map/ppermute | solution.py:18
  246.0 8.2 %slice-start = ((s8[6291456]{0:T(1024)(128)(4,1)}), s8[2097152]{0:T(1024)(128)(4,1)S(1)}, s32[]{:S(2)}) async-start(s8[6291456]{0:T(1024)(128)(4,1)} %bitcast.32), calls=%async_computation.4 | async-start | bytes 4194304
  250.6 3.7 %slice-start.1 = ((s8[6291456]{0:T(1024)(128)(4,1)}), s8[4194304]{0:T(1024)(128)(4,1)S(1)}, s32[]{:S(2)}) async-start(s8[6291456]{0:T(1024)(128)(4,1)} %bitcast.32), calls=%async_computation.5 | async-start | bytes 8388608
  255.2 5.4 %copy-start = (f32[8,256,512]{2,1,0:T(8,128)}, f32[8,256,512]{2,1,0:T(8,128)S(1)}, u32[]{:S(2)}) copy-start(f32[8,256,512]{2,1,0:T(8,128)S(1)} %fusion.1) | copy-start | bytes 12582916
  270.5 19.9 %all-to-all-start = ((bf16[4,256,512]{1,2,0:T(8,128)(2,1)}), bf16[4,256,512]{1,2,0:T(8,128)(2,1)S(1)}, u32[]{:S(2)}, u32[]{:S(2)}) async-start(bf16[4,256,512]{1,2,0:T(8,128)(2,1)} %broadcast_in_dim.45), calls=%async_computation | async-start | bytes 2097152 | tf_op jit(solution)/shard_map/all_to_all | solution.py:38
Sparse Core Ops, SparseCore 0:
  21.1 80.7 all-gather.5
  105.0 140.9 all-gather.3
  248.1 24.9 all-gather.7
where the time goes:
time: 304 us
  waiting for transfers between devices  191 us (63%)
  local copies, waits for them, and re-layouts  42.4 us (14%)
  matrix products  27.3 us (9%)
  blocking collectives  14.3 us (5%)
  between operations  13.4 us (4%)
  starting transfers between devices  9.79 us (3%)
  other arithmetic  5.19 us (2%)
    all_gather x1, waiting for transfers between devices, in_one_piece(): lax.all_gather(both, axis, axis=dim, tiled=True)  104 us
    all_gather x2, waiting for transfers between devices, gather_in_order(): pieces = lax.all_gather(pieces, axes[k], axis=0, tiled=True)  79.5 us
    all_gather x1, blocking collectives, gather_in_order(): pieces = lax.all_gather(pieces, axes[k], axis=0, tiled=True)  14.3 us
    reshape x1, local copies, waits for them, and re-layouts, banded_bias(): skewed = skewed.reshape(bias_table.shape[0], query_rows, span_len - 1)  12.4 us
    another operation x2, local copies, waits for them, and re-layouts, banded_bias(): repeated = jnp.tile(reversed_line, (1, query_rows))  11.9 us
    dot_general x1, matrix products, attend(): jnp.einsum('hqk,khe->qhe', weights_bf, values_all, preferred_element_type...  8.9 us
    transpose x1, local copies, waits for them, and re-layouts, gather_in_order(): pieces.transpose(*turned, *range(len(order), pieces.ndim))  8.25 us
    all_to_all x1, waiting for transfers between devices, from_everyone(): lax.all_to_all(jnp.broadcast_to(x[None], (length, *x.shape)), axis, 0, 0,...  7.32 us
  transfers between devices with their start and end apart: 6, of which 3 were waited for; matrix products, arithmetic and copies ran while one was open for 22% of the time, Pallas kernels for 0%

commit v1 on v0

--- a/solution.py
+++ b/solution.py
@@ -45,7 +45,9 @@
 def gather_in_order(x, axes, order):
     pieces = x[None]
     for k in order:
-        pieces = lax.all_gather(pieces, axes[k], axis=0, tiled=True)
+        pieces = jnp.concatenate(
+            lax.all_to_all(jnp.stack([pieces] * lax.axis_size(axes[k])), axes[k], 0, 0), axis=0
+        )
     held = [lax.axis_size(axes[k]) for k in reversed(order)]
     pieces = pieces.reshape(*held, *x.shape)
     turned = sorted(range(len(order)), key=lambda place: order[len(order) - 1 - place])

time: 304 us -> 331 us (1.089)
  the two profiles are of different devices: /device:TPU:32 before, /device:TPU:1 now
where the time goes in v1:
time: 331 us; the launch traced here: 330 us
  waiting for transfers between devices  179 us (54%)
  local copies, waits for them, and re-layouts  45.7 us (14%)
  blocking collectives  28.6 us (9%)
  starting transfers between devices  25.8 us (8%)
  matrix products  25.8 us (8%)
  between operations  13.7 us (4%)
  other arithmetic  11.9 us (4%)
    all_gather x1, waiting for transfers between devices, in_one_piece(): lax.all_gather(both, axis, axis=dim, tiled=True)  172 us
    all_to_all x2, blocking collectives, gather_in_order(): lax.all_to_all(jnp.stack([pieces] * lax.axis_size(axes[k])), axes[k], 0, 0)  28.6 us
    all_to_all x1, starting transfers between devices, gather_in_order(): lax.all_to_all(jnp.stack([pieces] * lax.axis_size(axes[k])), axes[k], 0, 0)  15.1 us
    reshape x1, local copies, waits for them, and re-layouts, banded_bias(): skewed = skewed.reshape(bias_table.shape[0], query_rows, span_len - 1)  12.3 us
    another operation x2, local copies, waits for them, and re-layouts, banded_bias(): repeated = jnp.tile(reversed_line, (1, query_rows))  11.9 us
    all_to_all x1, local copies, waits for them, and re-layouts, gather_in_order(): lax.all_to_all(jnp.stack([pieces] * lax.axis_size(axes[k])), axes[k], 0, 0)  8.28 us
    another operation x1, other arithmetic, gather_in_order(): jnp.stack([pieces] * lax.axis_size(axes[k]))  7.49 us
    dot_general x1, matrix products, attend(): jnp.einsum('hqk,khe->qhe', weights_bf, values_all, preferred_element_type...  7.45 us
  transfers between devices with their start and end apart: 5, of which 2 were waited for; matrix products, arithmetic and copies ran while one was open for 20% of the time, Pallas kernels for 0%

profile of v1, /device:TPU:1, one launch (start us, length us, event | category | flops | bytes accessed | tf_op | source)
XLA Modules:
  0.0 330.3 jit_solution(7637656796647401429)
XLA Ops:
  6.5 0.9 stack.9
  7.4 10.2 %all_to_all.20 = bf16[4,1,2048,16]{2,3,1,0:T(8,128)(2,1)S(1)} all-to-all(bf16[4,1,2048,16]{2,3,1,0:T(8,128)(2,1)S(1)} %stack.9), channel_id=1, replica_groups=mesh['sp_0'=16,'sp_1'=4,'sp_2'=2,'tp'=4] {'sp_1'}, dimensions={0} | all-to-all | bytes 524288 | tf_op jit(solution)/shard_map/all_to_all | solution.py:49
  17.6 2.5 stack.10
  20.1 0.0 copy-start.2
  20.1 0.0 copy-start.3
  20.1 0.0 copy-start.4
  20.1 0.0 copy-start.1
  20.1 0.0 copy-start.6
  20.1 0.0 copy-start.7
  20.1 0.0 copy-start.5
  20.1 15.1 %all-to-all-start.2 = ((bf16[16,4,2048,16]{2,3,1,0:T(8,128)(2,1)}), bf16[16,4,2048,16]{2,3,1,0:T(8,128)(2,1)}, u32[]{:S(2)}, u32[]{:S(2)}) async-start(bf16[16,4,2048,16]{2,3,1,0:T(8,128)(2,1)} %stack.10), calls=%async_computation.2 | async-start | bytes 8388608 | tf_op jit(solution)/shard_map/all_to_all | solution.py:49
  35.3 0.0 all-gather.2.cloned.1.call-start
  35.3 0.0 copy-done.2
  35.3 0.0 copy-done.3
  35.3 0.0 copy-done.4
  35.3 0.6 pad_maximum_fusion.8
  36.0 0.0 all-gather.2.cloned.1.call-update
  36.0 0.0 copy-done.1
  36.0 0.3 fusion.3
  36.3 0.0 copy-done.6
  36.3 1.3 fusion.5
  37.6 4.4 %collective-permute-start = (bf16[256,2048]{1,0:T(8,128)(2,1)}, bf16[256,2048]{1,0:T(8,128)(2,1)}, u32[]{:S(2)}, u32[]{:S(2)}) collective-permute-start(bf16[256,2048]{1,0:T(8,128)(2,1)} %fusion.5), channel_id=1, source_target_pairs={{0,4},{4,8},{8,12},{12,16},{16,20},{20,24},{24,28},{28,32},{32,36}... | collective-permute-start | bytes 3145736 | tf_op jit(solution)/shard_map/ppermute | solution.py:18
  42.0 0.0 copy-done.7
  42.0 1.9 collective-permute-start.1
  44.1 0.0 copy-done.5
  44.1 0.1 copy.18
  44.2 1.6 gather_fusion
  45.8 0.2 select_bitcast_fusion
  46.0 0.5 rev.3
  46.4 0.1 copy.19
  46.6 3.2 tile.4
  49.7 8.7 %tile.10 = f32[8,196352]{1,0:T(8,128)} reshape(f32[8,256,767]{2,1,0:T(8,128)} %tile.4) | data formatting | bytes 12566528 | tf_op jit(solution)/shard_map/tile | solution.py:67
  58.4 5.5 %slice.10 = f32[8,196096]{1,0:T(8,128)} slice(f32[8,196352]{1,0:T(8,128)} %tile.10), slice={[0:8], [255:196351]} | slice | bytes 12550144 | tf_op jit(solution)/shard_map/slice | solution.py:68
  63.9 12.3 %reshape.215 = f32[8,256,766]{2,1,0:T(8,128)} reshape(f32[8,196096]{1,0:T(8,128)} %slice.10) | data formatting | bytes 12550144 | tf_op jit(solution)/shard_map/reshape | solution.py:69
  76.2 0.0 collective-permute-done.1
  76.2 0.3 compare_and_fusion
  76.4 172.5 %all-gather.2.cloned.1.call-done = bf16[2048,1536]{1,0:T(8,128)(2,1)} async-done(((bf16[16,1536]{1,0:T(8,128)(2,1)}), bf16[2048,1536]{1,0:T(8,128)(2,1)}) %all-gather.2.cloned.1.call-update) | async-done | bytes 6291472 | tf_op jit(solution)/shard_map/all_gather | solution.py:27
  248.9 0.0 slice-start
  248.9 3.5 %fusion.20 = bf16[256,512]{1,0:T(8,128)(2,1)} fusion(bf16[256,2048]{1,0:T(8,128)(2,1)} %fusion.5, bf16[2048,1536]{1,0:T(8,128)(2,1)} %all-gather.2.cloned.1.call-done), kind=kOutput, calls=%fused_computation.25 | convolution fusion | flops 537001984 | bytes 3407872 | tf_op jit(solution)/shard_map/dot_general | solution.py:115
  252.4 1.1 copy.17
  253.5 0.0 slice-start.1
  253.5 0.0 collective-permute-done
  253.5 3.7 %fusion.16 = bf16[512,512]{0,1:T(8,128)(2,1)S(1)} fusion(bf16[2048,1536]{1,0:T(8,128)(2,1)} %all-gather.2.cloned.1.call-done, bf16[256,2048]{1,0:T(8,128)(2,1)} %fusion.5, bf16[256,2048]{1,0:T(8,128)(2,1)} %collective-permute-done), kind=kOutput, calls=%fused_computation.23 | convolution fusion | flops 1078198272 | bytes 4718592 | tf_op jit(solution)/shard_map/dot_general | solution.py:116
  257.2 0.0 slice-done
  257.2 0.0 slice-done.1
  257.2 0.9 fusion.1
  258.2 0.0 copy-start
  258.2 1.7 fusion.34
  259.9 3.5 %fusion.13 = bf16[512,512]{0,1:T(8,128)(2,1)S(1)} fusion(bf16[2048,1536]{1,0:T(8,128)(2,1)} %all-gather.2.cloned.1.call-done, bf16[256,2048]{1,0:T(8,128)(2,1)} %fusion.5, bf16[256,2048]{1,0:T(8,128)(2,1)} %collective-permute-done), kind=kOutput, calls=%fused_computation.22 | convolution fusion | flops 1078198272 | bytes 4718592 | tf_op jit(solution)/shard_map/dot_general | solution.py:117
  263.4 0.0 copy-done
  263.5 7.5 %fusion.19 = bf16[8,64,256]{2,1,0:T(8,128)(2,1)S(1)} fusion(bf16[512,8,64]{0,2,1:T(8,128)(2,1)S(1)} %bitcast.50, f32[8,256]{1,0:T(8,128)S(1)} %fusion.34, f32[8,256,512]{2,1,0:T(8,128)} %copy-done), kind=kOutput, calls=%fused_computation.24 | convolution fusion | flops 137497088 | bytes 4988928 | tf_op jit(solution)/shard_map/hqk,khe->qhe/dot_general | solution.py:93
  270.9 0.0 all-to-all-done.2
  270.9 7.5 %pad_maximum_fusion = bf16[2,64,2048,16]{2,3,1,0:T(8,128)(2,1)} fusion(bf16[1,64,2048,16]{2,3,1,0:T(8,128)(2,1)} %bitcast.15), kind=kLoop, calls=%fused_computation.2 | loop fusion | flops 4194304 | bytes 12582912 | tf_op jit(solution)/shard_map/stack | solution.py:49
  278.4 18.4 %all_to_all.21 = bf16[2,64,2048,16]{2,3,1,0:T(8,128)(2,1)} all-to-all(bf16[2,64,2048,16]{2,3,1,0:T(8,128)(2,1)} %pad_maximum_fusion), channel_id=1, replica_groups=mesh['sp_0'=16,'sp_1'=4,'sp_2'=2,'tp'=4] {'sp_2'}, dimensions={0} | all-to-all | bytes 16777216 | tf_op jit(solution)/shard_map/all_to_all | solution.py:49
  296.8 1.0 broadcast_in_dim.45
  297.9 4.3 %all-to-all-start = ((bf16[4,256,512]{1,2,0:T(8,128)(2,1)}), bf16[4,256,512]{1,2,0:T(8,128)(2,1)S(1)}, u32[]{:S(2)}, u32[]{:S(2)}) async-start(bf16[4,256,512]{1,2,0:T(8,128)(2,1)} %broadcast_in_dim.45), calls=%async_computation | async-start | bytes 2097152 | tf_op jit(solution)/shard_map/all_to_all | solution.py:38
  302.1 8.3 %copy.20 = bf16[2,64,2048,16]{2,3,0,1:T(8,128)(2,1)} copy(bf16[2,64,2048,16]{2,3,1,0:T(8,128)(2,1)} %all_to_all.21) | data formatting | bytes 16777216 | tf_op jit(solution)/shard_map/all_to_all | solution.py:49
  310.4 6.3 %all-to-all-done = bf16[4,256,512]{1,2,0:T(8,128)(2,1)S(1)} async-done(((bf16[4,256,512]{1,2,0:T(8,128)(2,1)}), bf16[4,256,512]{1,2,0:T(8,128)(2,1)S(1)}, u32[]{:S(2)}, u32[]{:S(2)}) %all-to-all-start) | async-done | bytes 1048608 | tf_op jit(solution)/shard_map/all_to_all | solution.py:38
  316.7 6.7 %fusion.2 = bf16[256,2048]{1,0:T(8,128)(2,1)} fusion(bf16[256,2048]{0,1:T(8,128)(2,1)S(1)} %bitcast.41, bf16[2048,2048]{0,1:T(8,128)(2,1)} %bitcast.38, bf16[256,2048]{1,0:T(8,128)(2,1)S(1)} %copy-done.1), kind=kOutput, calls=%fused_computation.10 | convolution fusion | flops 2149056512 | bytes 11534336 | tf_op jit(solution)/shard_map/dot_general | solution.py:135
  (9 shorter events, 0.1 us)
Async XLA Ops:
  20.1 15.2 %copy-start.2 = (bf16[1,16,512]{2,1,0:T(8,128)(2,1)S(1)}, bf16[1,16,512]{2,1,0:T(8,128)(2,1)}, u32[]{:S(2)}) copy-start(bf16[1,16,512]{2,1,0:T(8,128)(2,1)} %param.13) | copy-start | bytes 49156
  20.1 15.3 %copy-start.3 = (bf16[1,16,512]{2,1,0:T(8,128)(2,1)S(1)}, bf16[1,16,512]{2,1,0:T(8,128)(2,1)}, u32[]{:S(2)}) copy-start(bf16[1,16,512]{2,1,0:T(8,128)(2,1)} %param.12) | copy-start | bytes 49156
  20.1 15.3 %copy-start.4 = (bf16[1,16,512]{2,1,0:T(8,128)(2,1)S(1)}, bf16[1,16,512]{2,1,0:T(8,128)(2,1)}, u32[]{:S(2)}) copy-start(bf16[1,16,512]{2,1,0:T(8,128)(2,1)} %param.11) | copy-start | bytes 49156
  20.1 15.9 %copy-start.1 = (bf16[256,2048]{1,0:T(8,128)(2,1)S(1)}, bf16[256,2048]{1,0:T(8,128)(2,1)}, u32[]{:S(2)}) copy-start(bf16[256,2048]{1,0:T(8,128)(2,1)} %param.8) | copy-start | bytes 3145732
  20.1 16.2 %copy-start.6 = (f32[1,2048]{1,0:T(1,128)S(1)}, f32[1,2048]{1,0:T(1,128)}, u32[]{:S(2)}) copy-start(f32[1,2048]{1,0:T(1,128)} %param.10) | copy-start | bytes 24580
  20.1 21.9 %copy-start.7 = (s32[256]{0:T(256)S(1)}, s32[256]{0:T(256)}, u32[]{:S(2)}) copy-start(s32[256]{0:T(256)} %param.9) | copy-start | bytes 3076
  20.1 24.0 %copy-start.5 = (f32[1,8,257]{2,1,0:T(8,128)S(1)}, f32[1,8,257]{2,1,0:T(8,128)}, u32[]{:S(2)}) copy-start(f32[1,8,257]{2,1,0:T(8,128)} %param.15) | copy-start | bytes 24676
  20.1 250.8 %all-to-all-start.2 = ((bf16[16,4,2048,16]{2,3,1,0:T(8,128)(2,1)}), bf16[16,4,2048,16]{2,3,1,0:T(8,128)(2,1)}, u32[]{:S(2)}, u32[]{:S(2)}) async-start(bf16[16,4,2048,16]{2,3,1,0:T(8,128)(2,1)} %stack.10), calls=%async_computation.2 | async-start | bytes 8388608 | tf_op jit(solution)/shard_map/all_to_all | solution.py:49
  35.3 213.7 %all-gather.2.cloned.1.call-start = ((), (), s32[]{:S(2)}) async-start(), calls=%async_computation.4 | async-start | bytes 6340608 | tf_op jit(solution)/shard_map/all_gather | solution.py:27
  37.6 215.9 %collective-permute-start = (bf16[256,2048]{1,0:T(8,128)(2,1)}, bf16[256,2048]{1,0:T(8,128)(2,1)}, u32[]{:S(2)}, u32[]{:S(2)}) collective-permute-start(bf16[256,2048]{1,0:T(8,128)(2,1)} %fusion.5), channel_id=1, source_target_pairs={{0,4},{4,8},{8,12},{12,16},{16,20},{20,24},{24,28},{28,32},{32,36}... | collective-permute-start | bytes 3145736 | tf_op jit(solution)/shard_map/ppermute | solution.py:18
  42.0 34.1 %collective-permute-start.1 = (s32[256]{0:T(256)S(1)}, s32[256]{0:T(256)S(1)}, u32[]{:S(2)}, u32[]{:S(2)}) collective-permute-start(s32[256]{0:T(256)S(1)} %copy-done.7), channel_id=1, source_target_pairs={{0,4},{4,8},{8,12},{12,16},{16,20},{20,24},{24,28},{28,32},{32,36}... | collective-permute-start | bytes 3080 | tf_op jit(solution)/shard_map/ppermute | solution.py:18
  248.9 8.3 %slice-start = ((s8[6291456]{0:T(1024)(128)(4,1)}), s8[2097152]{0:T(1024)(128)(4,1)S(1)}, s32[]{:S(2)}) async-start(s8[6291456]{0:T(1024)(128)(4,1)} %bitcast.36), calls=%async_computation.5 | async-start | bytes 4194304
  253.5 3.7 %slice-start.1 = ((s8[6291456]{0:T(1024)(128)(4,1)}), s8[4194304]{0:T(1024)(128)(4,1)S(1)}, s32[]{:S(2)}) async-start(s8[6291456]{0:T(1024)(128)(4,1)} %bitcast.36), calls=%async_computation.6 | async-start | bytes 8388608
  258.2 5.3 %copy-start = (f32[8,256,512]{2,1,0:T(8,128)}, f32[8,256,512]{2,1,0:T(8,128)S(1)}, u32[]{:S(2)}) copy-start(f32[8,256,512]{2,1,0:T(8,128)S(1)} %fusion.1) | copy-start | bytes 12582916
  297.9 18.8 %all-to-all-start = ((bf16[4,256,512]{1,2,0:T(8,128)(2,1)}), bf16[4,256,512]{1,2,0:T(8,128)(2,1)S(1)}, u32[]{:S(2)}, u32[]{:S(2)}) async-start(bf16[4,256,512]{1,2,0:T(8,128)(2,1)} %broadcast_in_dim.45), calls=%async_computation | async-start | bytes 2097152 | tf_op jit(solution)/shard_map/all_to_all | solution.py:38
Sparse Core Ops, SparseCore 0:
  39.2 209.6 all-gather.1
